TPU v7x, 32 devices: a whole 2x2x4 slice. The times are simulated.
32 devices in a mesh: sp: 16 (over z, y, x), tp: 2 (over core).
Axes of the slice: x: 2, y: 2, z: 4, core: 2. Of those that a mesh axis runs over, the one named last changes fastest.
Arguments:
- resid: bfloat16 [3072, 2048], P('sp'), may hold values from -6 to 6
- query: bfloat16 [3072, 2048], P('sp', 'tp'), may hold values from -6 to 6
- key: bfloat16 [3072, 1024], P('sp', 'tp'), may hold values from -6 to 6
- value: bfloat16 [3072, 1024], P('sp', 'tp'), may hold values from -6 to 6
- q_gain: float32 [128], replicated, may hold values from 0.3 to 5, as said below
- k_gain: float32 [128], replicated, may hold values from 0.3 to 5, as said below
- out_weight: bfloat16 [2048, 2048], P('tp'), may hold values from -0.125 to 0.125
- norm_gain: float32 [2048], replicated, may hold values from 0.1 to 1.9
- gate_weight: bfloat16 [2048, 5632], P('sp', 'tp'), may hold values from -0.125 to 0.125
- up_weight: bfloat16 [2048, 5632], P('sp', 'tp'), may hold values from -0.125 to 0.125
- down_weight: bfloat16 [5632, 2048], P('tp', 'sp'), may hold values from -0.078125 to 0.078125
Outputs:
- mixed: bfloat16 [3072, 2048], P(('sp', 'tp'))
Inputs may be any that keep to these rules, and one draw needn't show every extreme that they name: `q_gain`: positive gains. `k_gain`: positive gains.
All inputs are finite; a program needn't handle non-finite values.
Results may differ from a plain program's by a relative error of at most 0.012.
The roundings to bfloat16 on the way count: a program that leaves them out, or rounds other values in their place, can miss the bound.
Values may be sent and summed in bfloat16 or wider, within the bound.
A program may use at most 128 MiB of HBM per device.

v0:
```python
import jax
import jax.numpy as jnp
from jax import lax
from jax.sharding import PartitionSpec as P

GRID_W = 64
EPSILON = 1e-06


def rotate(values, positions):
    dim_size = values.shape[-1]
    half_dim = dim_size // 2
    quarter = half_dim // 2
    inverse = 10000.0 ** (-jnp.arange(quarter, dtype=jnp.float32) / quarter)
    outputs = []
    for axis_pos, coords in enumerate((positions // GRID_W, positions % GRID_W)):
        angles = coords.astype(jnp.float32)[:, None] * inverse[None, :]
        cosine = jnp.cos(angles)[:, None, :]
        sine = jnp.sin(angles)[:, None, :]
        section = values[..., axis_pos * half_dim : (axis_pos + 1) * half_dim]
        first_half = section[..., :quarter]
        second_half = section[..., quarter:]
        outputs += [
            first_half * cosine - second_half * sine,
            second_half * cosine + first_half * sine,
        ]
    return jnp.concatenate(outputs, axis=-1)


def prepare(projected, gain, positions):
    values = projected.astype(jnp.float32)
    normed = values * lax.rsqrt(jnp.mean(values * values, axis=-1, keepdims=True) + EPSILON) * gain
    return rotate(normed, positions).astype(jnp.bfloat16)


def normalize(stream, gain):
    values = stream.astype(jnp.float32)
    return (
        values * lax.rsqrt(jnp.mean(values * values, axis=-1, keepdims=True) + EPSILON) * gain
    ).astype(jnp.bfloat16)


def body(
    resid,
    query,
    key,
    value,
    q_gain,
    k_gain,
    out_weight,
    norm_gain,
    gate_weight,
    up_weight,
    down_weight,
):
    rows_here = query.shape[0]
    head_dim = q_gain.shape[0]
    heads_here = query.shape[1] // head_dim
    kv_here = key.shape[1] // head_dim
    group_size = heads_here // kv_here
    score_scale = head_dim ** (-0.5)
    positions = lax.axis_index("sp") * rows_here + jnp.arange(rows_here, dtype=jnp.int32)
    q_rot = prepare(query.reshape(rows_here, heads_here, head_dim), q_gain, positions)
    k_rot = prepare(key.reshape(rows_here, kv_here, head_dim), k_gain, positions)
    val_rows = value.reshape(rows_here, kv_here, head_dim)
    grouped = q_rot.reshape(rows_here, kv_here, group_size, head_dim)

    def key_block(carry, block):
        maxima, totals, accum = carry
        block_keys, block_vals = block
        scores = (
            jnp.einsum("qkgd,skd->kgqs", grouped, block_keys, preferred_element_type=jnp.float32)
            * score_scale
        )
        new_max = jnp.maximum(maxima, jnp.max(scores, axis=-1))
        shrink = jnp.exp(maxima - new_max)
        weights = jnp.exp(scores - new_max[..., None])
        totals = totals * shrink + jnp.sum(weights, axis=-1)
        accum = accum * shrink[..., None] + jnp.einsum(
            "kgqs,skd->kgqd",
            weights.astype(jnp.bfloat16),
            block_vals,
            preferred_element_type=jnp.float32,
        )
        return ((new_max, totals, accum), None)

    start_max = jnp.full((kv_here, group_size, rows_here), -1e30, jnp.float32)
    start_total = jnp.zeros((kv_here, group_size, rows_here), jnp.float32)
    start_accum = jnp.zeros((kv_here, group_size, rows_here, head_dim), jnp.float32)
    carry = (start_max, start_total, start_accum)
    key_part = lax.all_gather(k_rot, "sp", axis=0, tiled=True)
    val_part = lax.all_gather(val_rows, "sp", axis=0, tiled=True)
    length = key_part.shape[0]
    factor = 4
    span = rows_here * factor
    turns = length // span
    key_blocks = key_part.reshape(turns, span, kv_here, head_dim)
    val_blocks = val_part.reshape(turns, span, kv_here, head_dim)
    carry, _ = lax.scan(key_block, carry, (key_blocks, val_blocks))
    maxima, totals, accum = carry
    attn = (
        jnp.transpose(accum / totals[..., None], (2, 0, 1, 3))
        .reshape(rows_here, heads_here * head_dim)
        .astype(jnp.bfloat16)
    )
    share = rows_here // lax.axis_size("tp")
    my_first = lax.axis_index("tp") * share
    proj = lax.psum_scatter(
        jnp.dot(attn, out_weight, preferred_element_type=jnp.float32).astype(jnp.bfloat16),
        "tp",
        scatter_dimension=0,
        tiled=True,
    ).astype(jnp.float32)
    my_resid = lax.dynamic_slice_in_dim(resid, my_first, share, 0)
    my_stream = (my_resid.astype(jnp.float32) + proj).astype(jnp.bfloat16)
    mixer_rows = lax.all_gather(normalize(my_stream, norm_gain), "tp", axis=0, tiled=True)

    def add_rows(shard_rows):
        return jnp.dot(mixer_rows, shard_rows, preferred_element_type=jnp.float32)

    gate = add_rows(lax.all_gather(gate_weight, "sp", axis=0, tiled=True))
    up_part = add_rows(lax.all_gather(up_weight, "sp", axis=0, tiled=True))
    hidden = (jax.nn.silu(gate) * up_part).astype(jnp.bfloat16)
    down_whole = lax.all_gather(down_weight, "sp", axis=1, tiled=True)
    down = lax.psum_scatter(
        jnp.dot(hidden, down_whole, preferred_element_type=jnp.float32).astype(jnp.bfloat16),
        "tp",
        scatter_dimension=0,
        tiled=True,
    ).astype(jnp.float32)
    return (my_stream.astype(jnp.float32) + 0.5 * down).astype(jnp.bfloat16)


def solution(mesh):
    placed = (
        P("sp", None),
        P("sp", "tp"),
        P("sp", "tp"),
        P("sp", "tp"),
        P(),
        P(),
        P("tp", None),
        P(),
        P("sp", "tp"),
        P("sp", "tp"),
        P("tp", "sp"),
    )
    return jax.shard_map(
        body, mesh=mesh, in_specs=placed, out_specs=P(("sp", "tp"), None), check_vma=False
    )
```

profile of v0, /device:TPU:0, one launch (start us, length us, event | category | flops | bytes accessed | tf_op | source)
XLA Modules:
  0.0 702.4 jit_solution(25329568361684075)
XLA Ops:
  15.1 67.4 %all-gather.6.cloned.1.call-done = bf16[3072,4,128]{2,1,0:T(4,128)(2,1)} async-done(((bf16[192,4,128]{2,1,0:T(4,128)(2,1)}), bf16[3072,4,128]{2,1,0:T(4,128)(2,1)}) %all-gather.6.cloned.1.call-update) | async-done | bytes 3145744 | tf_op jit(solution)/shard_map/all_gather | solution.py:91
  82.5 69.2 %all-gather.8.cloned.1.call-done = bf16[3072,4,128]{2,1,0:T(4,128)(2,1)} async-done(((bf16[192,4,128]{2,1,0:T(4,128)(2,1)}), bf16[3072,4,128]{2,1,0:T(4,128)(2,1)}) %all-gather.8.cloned.1.call-update) | async-done | bytes 3145744 | tf_op jit(solution)/shard_map/all_gather | solution.py:92
  151.7 40.1 %while.15 = (s32[]{:T(128)}, f32[4,2,192]{2,1,0:T(2,128)S(1)}, f32[4,2,192]{2,1,0:T(2,128)S(1)}, f32[4,2,192,128]{3,2,1,0:T(8,128)S(1)}, bf16[4,768,4,128]{3,2,1...) while((s32[]{:T(128)}, f32[4,2,192]{2,1,0:T(2,128)S(1)}, ...), condition=%wide.region_5.6_spmd.clone, body=%wide.region_2.5_spmd.clone.sunk | while | flops 614014464 | bytes 39813256 | solution.py:99
  151.7 1.9 constant_dynamic-slice_fusion.3
  153.6 2.9 bitcast_reduce_fusion.2
  156.5 3.5 fusion.42
  161.7 1.9 constant_dynamic-slice_fusion.3
  163.6 2.9 bitcast_reduce_fusion.2
  166.6 3.5 fusion.42
  171.7 1.9 constant_dynamic-slice_fusion.3
  173.6 2.9 bitcast_reduce_fusion.2
  176.6 3.5 fusion.42
  181.7 1.9 constant_dynamic-slice_fusion.3
  183.7 2.9 bitcast_reduce_fusion.2
  186.6 3.5 fusion.42
  192.8 4.1 convolution_convert_fusion.1
  198.7 5.1 reduce-scatter.3.cloned.1.call-done
  205.2 2.5 all_gather.20
  207.7 141.2 %all-gather.10.cloned.1.call-done = bf16[2048,2816]{1,0:T(8,128)(2,1)} async-done(((bf16[128,2816]{1,0:T(8,128)(2,1)}), bf16[2048,2816]{1,0:T(8,128)(2,1)}) %all-gather.10.cloned.1.call-update) | async-done | bytes 11534352 | tf_op jit(solution)/shard_map/all_gather | solution.py:121
  348.9 6.7 fusion.24
  355.6 135.6 %all-gather.12.cloned.1.call-done = bf16[2048,2816]{1,0:T(8,128)(2,1)} async-done(((bf16[128,2816]{1,0:T(8,128)(2,1)}), bf16[2048,2816]{1,0:T(8,128)(2,1)}) %all-gather.12.cloned.1.call-update) | async-done | bytes 11534352 | tf_op jit(solution)/shard_map/all_gather | solution.py:122
  491.2 182.8 %all-gather.14.cloned.1.call-done = bf16[2816,2048]{1,0:T(8,128)(2,1)} async-done(((bf16[2816,128]{1,0:T(8,128)(2,1)}), bf16[2816,2048]{1,0:T(8,128)(2,1)}) %all-gather.14.cloned.1.call-update) | async-done | bytes 11534352 | tf_op jit(solution)/shard_map/all_gather | solution.py:124
  674.0 13.2 %convolution_convert_fusion = bf16[192,2048]{1,0:T(8,128)(2,1)} fusion(bf16[2816,2048]{1,0:T(8,128)(2,1)} %all-gather.14.cloned.1.call-done, bf16[192,2048]{1,0:T(8,128)(2,1)S(1)} %all_gather.20, bf16[2048,2816]{1,0:T(8,128)(2,1)} %all-gather.12.cloned.1.call-done, f32[192,2816]{1,0:T(8,128)S(1)} %fusion.24), kind=kOutput, calls=%fused_computation.23 | convolution fusion | flops 4432822272 | bytes 26804224 | tf_op jit(solution)/shard_map/dot_general | solution.py:126
  687.2 6.5 reduce-scatter.5.cloned.1.call-done
  (81 shorter events, 20.8 us)
Async XLA Ops:
  6.5 5.2 copy-start.2
  6.5 6.1 copy-start.1
  6.5 75.9 %all-gather.6.cloned.1.call-start = ((), (), s32[]{:S(2)}) async-start(), calls=%async_computation.2 | async-start | bytes 3342336 | tf_op jit(solution)/shard_map/all_gather | solution.py:91
  8.0 5.3 copy-start.5
  11.7 140.0 %all-gather.8.cloned.1.call-start = ((), (), s32[]{:S(2)}) async-start(), calls=%async_computation.3 | async-start | bytes 3342336 | tf_op jit(solution)/shard_map/all_gather | solution.py:92
  12.5 191.2 %reduce-scatter.3.cloned.1.call-start = ((), (), s32[]{:S(2)}) async-start(), calls=%async_computation.4 | async-start | bytes 1179648 | tf_op jit(solution)/shard_map/reduce_scatter | solution.py:108
  156.5 3.8 copy-start
  166.5 3.8 copy-start
  176.6 3.8 copy-start
  186.6 3.8 copy-start
  192.5 11.3 %copy-start.3 = (bf16[192,2048]{1,0:T(8,128)(2,1)S(1)}, bf16[192,2048]{1,0:T(8,128)(2,1)}, u32[]{:S(2)}) copy-start(bf16[192,2048]{1,0:T(8,128)(2,1)} %param.13) | copy-start | bytes 2359300
  192.7 12.3 %copy-start.4 = (f32[2048]{0:T(1024)S(1)}, f32[2048]{0:T(1024)}, u32[]{:S(2)}) copy-start(f32[2048]{0:T(1024)} %param.20) | copy-start | bytes 24580
  196.9 152.0 %all-gather.10.cloned.1.call-start = ((), (), s32[]{:S(2)}) async-start(), calls=%async_computation.5 | async-start | bytes 12255232 | tf_op jit(solution)/shard_map/all_gather | solution.py:121
  197.5 293.7 %all-gather.12.cloned.1.call-start = ((), (), s32[]{:S(2)}) async-start(), calls=%async_computation.6 | async-start | bytes 12255232 | tf_op jit(solution)/shard_map/all_gather | solution.py:122
  198.1 475.9 %all-gather.14.cloned.1.call-start = ((), (), s32[]{:S(2)}) async-start(), calls=%async_computation.7 | async-start | bytes 12255232 | tf_op jit(solution)/shard_map/all_gather | solution.py:124
  198.6 495.1 %reduce-scatter.5.cloned.1.call-start = ((), (), s32[]{:S(2)}) async-start(), calls=%async_computation.8 | async-start | bytes 1179648 | tf_op jit(solution)/shard_map/reduce_scatter | solution.py:125
Sparse Core Ops, SparseCore 0:
  11.9 70.5 all-gather.5
  85.2 66.3 all-gather.7
  197.0 6.6 reduce-scatter.2
  206.4 142.5 all-gather.9
  351.5 139.5 all-gather.11
  493.7 180.2 all-gather.13
  687.3 6.3 reduce-scatter.4
where the time goes:
time: 703 us; the launch traced here: 702 us
  waiting for transfers between devices  609 us (87%)
  matrix products  41.2 us (6%)
  other arithmetic  23.7 us (3%)
  between operations  13.8 us (2%)
  local copies, waits for them, and re-layouts  11.4 us (2%)
    all_gather x1, waiting for transfers between devices, body(): down_whole = lax.all_gather(down_weight, 'sp', axis=1, tiled=True)  183 us
    all_gather x1, waiting for transfers between devices, body(): gate = add_rows(lax.all_gather(gate_weight, 'sp', axis=0, tiled=True))  141 us
    all_gather x1, waiting for transfers between devices, body(): up_part = add_rows(lax.all_gather(up_weight, 'sp', axis=0, tiled=True))  136 us
    all_gather x1, waiting for transfers between devices, body(): val_part = lax.all_gather(val_rows, 'sp', axis=0, tiled=True)  69.2 us
    all_gather x1, waiting for transfers between devices, body(): key_part = lax.all_gather(k_rot, 'sp', axis=0, tiled=True)  67.4 us
    reduce_sum x4, other arithmetic, key_block(): totals = totals * shrink + jnp.sum(weights, axis=-1)  14.2 us
  transfers between devices with their start and end apart: 7, of which 7 were waited for; matrix products, arithmetic and copies ran while one was open for 2% of the time, Pallas kernels for 0%

commit v1 on v0

--- a/solution.py
+++ b/solution.py
@@ -88,8 +88,11 @@
     start_total = jnp.zeros((kv_here, group_size, rows_here), jnp.float32)
     start_accum = jnp.zeros((kv_here, group_size, rows_here, head_dim), jnp.float32)
     carry = (start_max, start_total, start_accum)
-    key_part = lax.all_gather(k_rot, "sp", axis=0, tiled=True)
-    val_part = lax.all_gather(val_rows, "sp", axis=0, tiled=True)
+    key_part, val_part = jnp.split(
+        lax.all_gather(jnp.concatenate([k_rot, val_rows], axis=1), "sp", axis=0, tiled=True),
+        [k_rot.shape[1]],
+        axis=1,
+    )
     length = key_part.shape[0]
     factor = 4
     span = rows_here * factor

time: 703 us -> 673 us (0.957)
  waiting for transfers between devices: 609 us -> 567 us
  matrix products: 41.2 us -> 49.7 us
    all_gather x2 -> x1, waiting for transfers between devices: 137 us -> 93.7 us  [body(): lax.all_gather(jnp.concatenate([k_rot, val_rows], axis=1), 'sp', axis=0,...]
    dynamic_slice x4 -> x0, local copies, waits for them, and re-layouts: 7.66 us -> none  [body(): carry, _ = lax.scan(key_block, carry, (key_blocks, val_blocks))]
    split x0 -> x1, local copies, waits for them, and re-layouts: none -> 7.09 us  [body(): jnp.split(lax.all_gather(jnp.concatenate([k_rot, val_rows], axis=1), 'sp'...]
  transfers between devices with their start and end apart: 7 -> 6, of which waited for: 7 -> 6; matrix products, arithmetic and copies ran while one was open for 2% -> 2% of each run, Pallas kernels for 0% -> 0%
where the time goes in v1:
time: 673 us; the launch traced here: 672 us
  waiting for transfers between devices  567 us (84%)
  matrix products  49.7 us (7%)
  other arithmetic  23.9 us (4%)
  local copies, waits for them, and re-layouts  15.3 us (2%)
  between operations  13.7 us (2%)
    all_gather x1, waiting for transfers between devices, body(): down_whole = lax.all_gather(down_weight, 'sp', axis=1, tiled=True)  176 us
    all_gather x1, waiting for transfers between devices, body(): up_part = add_rows(lax.all_gather(up_weight, 'sp', axis=0, tiled=True))  142 us
    all_gather x1, waiting for transfers between devices, body(): gate = add_rows(lax.all_gather(gate_weight, 'sp', axis=0, tiled=True))  142 us
    all_gather x1, waiting for transfers between devices, body(): lax.all_gather(jnp.concatenate([k_rot, val_rows], axis=1), 'sp', axis=0,...  93.7 us
    dot_general x4, matrix products, key_block(): jnp.einsum('qkgd,skd->kgqs', grouped, block_keys, preferred_element_type=...  16.2 us
    reduce_sum x4, other arithmetic, key_block(): totals = totals * shrink + jnp.sum(weights, axis=-1)  14.2 us
  transfers between devices with their start and end apart: 6, of which 6 were waited for; matrix products, arithmetic and copies ran while one was open for 2% of the time, Pallas kernels for 0%

profile of v1, /device:TPU:0, one launch (start us, length us, event | category | flops | bytes accessed | tf_op | source)
XLA Modules:
  0.0 672.1 jit_solution(14385280073637313155)
XLA Ops:
  15.5 93.7 %all-gather.5.cloned.1.call-done = bf16[3072,8,128]{2,1,0:T(8,128)(2,1)} async-done(((bf16[192,8,128]{2,1,0:T(8,128)(2,1)}), bf16[3072,8,128]{2,1,0:T(8,128)(2,1)}) %all-gather.5.cloned.1.call-update) | async-done | bytes 6291472 | tf_op jit(solution)/shard_map/all_gather | solution.py:92
  109.2 7.1 %fusion.30 = (bf16[3072,4,128]{2,1,0:T(4,128)(2,1)S(1)}, bf16[3072,4,128]{2,1,0:T(4,128)(2,1)S(1)}) fusion(bf16[3072,8,128]{2,1,0:T(8,128)(2,1)} %all-gather.5.cloned.1.call-done), kind=kLoop, calls=%fused_computation.71 | loop fusion | bytes 12582912 | tf_op jit(solution)/shard_map/split | solution.py:91
  120.5 40.8 %while.15 = (s32[]{:T(128)}, f32[4,2,192]{2,1,0:T(2,128)S(1)}, f32[4,2,192]{2,1,0:T(2,128)S(1)}, f32[4,2,192,128]{3,2,1,0:T(8,128)S(1)}, bf16[4,768,4,128]{3,1,0...) while((s32[]{:T(128)}, f32[4,2,192]{2,1,0:T(2,128)S(1)}, ...), condition=%wide.region_5.6_spmd.clone, body=%wide.region_2.5_spmd.clone.sunk | while | flops 614014464 | bytes 36668548 | solution.py:102
  120.5 4.0 bitcast_reduce_fusion.2
  124.5 3.5 fusion.51
  128.3 2.4 fusion.53
  130.7 4.1 bitcast_reduce_fusion.2
  134.7 3.5 fusion.51
  138.5 2.4 fusion.53
  140.9 4.1 bitcast_reduce_fusion.2
  145.0 3.5 fusion.51
  148.7 2.4 fusion.53
  151.1 4.1 bitcast_reduce_fusion.2
  155.2 3.5 fusion.51
  158.9 2.4 fusion.53
  162.3 4.1 convolution_convert_fusion.1
  168.6 4.7 reduce-scatter.3.cloned.1.call-done
  174.7 2.4 all_gather.16
  177.1 141.5 %all-gather.7.cloned.1.call-done = bf16[2048,2816]{1,0:T(8,128)(2,1)} async-done(((bf16[128,2816]{1,0:T(8,128)(2,1)}), bf16[2048,2816]{1,0:T(8,128)(2,1)}) %all-gather.7.cloned.1.call-update) | async-done | bytes 11534352 | tf_op jit(solution)/shard_map/all_gather | solution.py:124
  318.6 6.7 fusion.31
  325.3 176.1 %all-gather.11.cloned.1.call-done = bf16[2816,2048]{1,0:T(8,128)(2,1)} async-done(((bf16[2816,128]{1,0:T(8,128)(2,1)}), bf16[2816,2048]{1,0:T(8,128)(2,1)}) %all-gather.11.cloned.1.call-update) | async-done | bytes 11534352 | tf_op jit(solution)/shard_map/all_gather | solution.py:127
  501.4 142.2 %all-gather.9.cloned.1.call-done = bf16[2048,2816]{1,0:T(8,128)(2,1)} async-done(((bf16[128,2816]{1,0:T(8,128)(2,1)}), bf16[2048,2816]{1,0:T(8,128)(2,1)}) %all-gather.9.cloned.1.call-update) | async-done | bytes 11534352 | tf_op jit(solution)/shard_map/all_gather | solution.py:125
  643.7 13.2 %convolution_convert_fusion = bf16[192,2048]{1,0:T(8,128)(2,1)} fusion(bf16[2816,2048]{1,0:T(8,128)(2,1)} %all-gather.11.cloned.1.call-done, bf16[192,2048]{1,0:T(8,128)(2,1)S(1)} %all_gather.16, bf16[2048,2816]{1,0:T(8,128)(2,1)} %all-gather.9.cloned.1.call-done, f32[192,2816]{1,0:T(8,128)S(1)} %fusion.31), kind=kOutput, calls=%fused_computation.25 | convolution fusion | flops 4432822272 | bytes 26804224 | tf_op jit(solution)/shard_map/dot_general | solution.py:129
  656.9 6.5 reduce-scatter.5.cloned.1.call-done
  (75 shorter events, 20.1 us)
Async XLA Ops:
  6.5 6.4 copy-start.1
  6.5 102.6 %all-gather.5.cloned.1.call-start = ((), (), s32[]{:S(2)}) async-start(), calls=%async_computation.2 | async-start | bytes 6684672 | tf_op jit(solution)/shard_map/all_gather | solution.py:92
  9.0 4.7 copy-start.4
  12.9 160.4 %reduce-scatter.3.cloned.1.call-start = ((), (), s32[]{:S(2)}) async-start(), calls=%async_computation.3 | async-start | bytes 1179648 | tf_op jit(solution)/shard_map/reduce_scatter | solution.py:111
  124.5 3.8 copy-start
  134.7 3.8 copy-start
  144.9 3.8 copy-start
  155.2 3.8 copy-start
  162.0 11.3 %copy-start.2 = (bf16[192,2048]{1,0:T(8,128)(2,1)S(1)}, bf16[192,2048]{1,0:T(8,128)(2,1)}, u32[]{:S(2)}) copy-start(bf16[192,2048]{1,0:T(8,128)(2,1)} %param.13) | copy-start | bytes 2359300
  162.3 12.3 %copy-start.3 = (f32[2048]{0:T(1024)S(1)}, f32[2048]{0:T(1024)}, u32[]{:S(2)}) copy-start(f32[2048]{0:T(1024)} %param.20) | copy-start | bytes 24580
  166.4 152.2 %all-gather.7.cloned.1.call-start = ((), (), s32[]{:S(2)}) async-start(), calls=%async_computation.4 | async-start | bytes 12255232 | tf_op jit(solution)/shard_map/all_gather | solution.py:124
  167.2 334.3 %all-gather.11.cloned.1.call-start = ((), (), s32[]{:S(2)}) async-start(), calls=%async_computation.6 | async-start | bytes 12255232 | tf_op jit(solution)/shard_map/all_gather | solution.py:127
  167.8 475.9 %all-gather.9.cloned.1.call-start = ((), (), s32[]{:S(2)}) async-start(), calls=%async_computation.5 | async-start | bytes 12255232 | tf_op jit(solution)/shard_map/all_gather | solution.py:125
  168.3 495.1 %reduce-scatter.5.cloned.1.call-start = ((), (), s32[]{:S(2)}) async-start(), calls=%async_computation.7 | async-start | bytes 1179648 | tf_op jit(solution)/shard_map/reduce_scatter | solution.py:128
Sparse Core Ops, SparseCore 0:
  13.0 96.1 all-gather.4
  166.6 6.6 reduce-scatter.2
  176.1 142.5 all-gather.6
  321.2 180.2 all-gather.10
  504.0 139.5 all-gather.8
  657.0 6.3 reduce-scatter.4
